TPU v7x, 128 devices: a whole 4x4x4 slice. The times are simulated.
128 devices in a mesh: rep: 2 (over z_hi), fs: 32 (over z_lo, y, x), tp: 2 (over core).
Axes of the slice: x: 4, y: 4, z: 4 (z_hi: 2, z_lo: 2; z = z_hi * 2 + z_lo), core: 2. Of those that a mesh axis runs over, the one named last changes fastest.
Arguments:
- inputs: bfloat16 [32768, 1024], P(('rep', 'fs', 'tp')), may hold values from -6 to 6
- up_proj: bfloat16 [1024, 4096], P('fs', 'tp'), may hold values from -0.1875 to 0.1875
- down_proj: bfloat16 [4096, 1024], P('tp', 'fs'), may hold values from -0.09375 to 0.09375
- out_cotangent: bfloat16 [32768, 1024], P(('rep', 'fs', 'tp')), may hold values from -24 to 24
Outputs:
- grad_inputs: bfloat16 [32768, 1024], P(('rep', 'fs', 'tp'))
- grad_up: float32 [1024, 4096], P('fs', 'tp')
- grad_down: float32 [4096, 1024], P('tp', 'fs')
- energy_up: float32 [1024], P('fs')
- energy_down: float32 [4096], P('tp')
All inputs are finite; a program needn't handle non-finite values.
Results may differ from a plain program's by a relative error of at most 0.001.
Values may be sent and summed in bfloat16 or wider, within the bound.
A program may use at most 128 MiB of HBM per device.

v0:
```python
import functools

import jax
import jax.numpy as jnp
from jax import lax
from jax.experimental import pallas as pl
from jax.experimental.pallas import tpu as pltpu
from jax.sharding import PartitionSpec as P

MESH = pl.DeviceIdType.MESH
ORDERS = (
    (0, 4, 1, 2, 3),
    (2, 3, 4, 0, 1),
    (1, 0, 3, 4, 2),
    (3, 2, 1, 4, 0),
    (3, 0, 2, 4, 1),
    (2, 1, 0, 4, 3),
    (0, 1, 4, 3, 2),
    (3, 2, 1, 4, 0),
)
STEPS = 5
PARTS = len(ORDERS)


def bits_of(fs):
    z, y, x = fs // 16, (fs // 4) % 4, fs % 4
    return (z, (y % 2 + y // 2) % 2, y // 2, (x % 2 + x // 2) % 2, x // 2)


def partners_of(fs):
    z, y, x = fs // 16, (fs // 4) % 4, fs % 4
    return (
        fs + 16 - 32 * z,
        fs + 4 - 8 * (y % 2),
        fs + 12 - 8 * y,
        fs + 1 - 2 * (x % 2),
        fs + 3 - 2 * x,
    )


def remote(src, dst, send, recv, device):
    return pltpu.make_async_remote_copy(
        src_ref=src, dst_ref=dst, send_sem=send, recv_sem=recv, device_id=device, device_id_type=MESH
    )


def contract(left, right, left_dim, right_dim):
    return lax.dot_general(
        left, right, (((left_dim,), (right_dim,)), ((), ())), preferred_element_type=jnp.float32
    )


def kernel(
    factor,
    x_ref,
    c_ref,
    u_ref,
    d_ref,
    gin_ref,
    gup_ref,
    gdn_ref,
    eup_ref,
    edn_ref,
    tok,
    tokt,
    wg,
    wn,
    pre,
    act,
    gpre,
    gbuf,
    rbuf,
    part_in,
    pair_in,
    last_in,
    outs,
    ebuf,
    esum,
    eup_own,
    eup_in,
    tok_s,
    tok_r,
    fwd_s,
    fwd_r,
    sib_s,
    sib_r,
    g_s,
    g_r,
    r_s,
    r_r,
    rep_s,
    rep_r,
    pi_s,
    pi_r,
    li_s,
    li_r,
    e_s,
    e_r,
    eu_s,
    eu_r,
):
    rep, fs, tp = lax.axis_index("rep"), lax.axis_index("fs"), lax.axis_index("tp")
    mine = bits_of(fs)
    near = [{"fs": other} for other in partners_of(fs)]
    sibling = {"tp": 1 - tp}
    pair = {"rep": 1 - rep, "fs": partners_of(fs)[0]}
    twin = {"rep": 1 - rep}
    rows, width = x_ref.shape
    shard = u_ref.shape[0]
    hidden = u_ref.shape[1] // 2
    cols = hidden // PARTS
    base = rep * hidden
    weights = (u_ref, d_ref)
    tokens = (x_ref, c_ref)
    pieces = 2
    chunk = rows // pieces

    barrier = pltpu.get_barrier_semaphore()
    for device in near + [sibling, pair, twin]:
        pl.semaphore_signal(barrier, inc=1, device_id=device, device_id_type=MESH)

    for m in range(2):
        tok[m, 0] = tokens[m][...]
        for p in range(PARTS):
            wg[m, p, 0] = weights[m][:, pl.ds(pl.multiple_of(base + p * cols, cols), cols)]

    pl.semaphore_wait(barrier, STEPS + 3)

    pending = []

    def start(copy):
        copy.start()
        pending.append(copy)
        return copy

    def token_copy(m, q):
        return remote(
            tokens[m].at[pl.ds(q * chunk, chunk)],
            tok.at[m, 2, pl.ds(q * chunk, chunk)],
            tok_s.at[m, q],
            tok_r.at[m, q],
            pair,
        )

    def forward_copy(m, q):
        return remote(
            tok.at[m, 2, pl.ds(q * chunk, chunk)],
            tok.at[m, 3, pl.ds(q * chunk, chunk)],
            fwd_s.at[m, q],
            fwd_r.at[m, q],
            sibling,
        )

    def sibling_copy(m):
        return remote(tokens[m], tok.at[m, 1], sib_s.at[m], sib_r.at[m], sibling)

    def gather_copy(m, p, k):
        if k == 0:
            src = weights[m].at[:, pl.ds(pl.multiple_of(base + p * cols, cols), cols)]
            dst = wg.at[m, p, 1]
        else:
            src = wg.at[m, p, pl.ds(0, 2**k)]
            dst = wg.at[m, p, pl.ds(2**k, 2**k)]
        return remote(src, dst, g_s.at[m * PARTS + p, k], g_r.at[m * PARTS + p, k], near[ORDERS[p][k]])

    def gather_step(m, k):
        for p in range(PARTS):
            if k > 0:
                gather_copy(m, p, k - 1).wait_recv()
            start(gather_copy(m, p, k))

    def forward(m, q):
        token_copy(m, q).wait_recv()
        start(forward_copy(m, q))

    for m in range(2):
        gather_step(m, 0)
        for q in range(pieces):
            start(token_copy(m, q))
    for m in range(2):
        start(sibling_copy(m))

    def transpose(m, g):
        tokt[m, :, g * rows : (g + 1) * rows] = tok[m, g].T

    gather_step(0, 1)
    gather_step(1, 1)
    gather_step(0, 2)
    gather_step(1, 2)
    for m in range(2):
        transpose(m, 0)
        sibling_copy(m).wait_recv()
        transpose(m, 1)
    forward(0, 0)
    gather_step(0, 3)
    gather_step(1, 3)
    forward(0, 1)
    gather_step(0, 4)
    gather_step(1, 4)

    def slot(bits, p):
        total = 0
        for k in range(STEPS):
            total = total + bits[ORDERS[p][k]] * 2**k
        return total

    def relative(shard_index):
        return [(a + b) % 2 for a, b in zip(mine, bits_of(shard_index))]

    def unpack(m, p):
        gather_copy(m, p, STEPS - 1).wait_recv()

        def some(i, carry):
            for t in range(8):
                s = i * 8 + t
                wn[m, pl.ds(pl.multiple_of(s * shard, shard), shard), p * cols : (p + 1) * cols] = wg[
                    m, p, slot(relative(s), p)
                ]
            return carry

        lax.fori_loop(0, 4, some, 0)

    for q in range(pieces):
        forward_copy(0, q).wait_recv()
    transpose(0, 2)
    transpose(0, 3)
    blocks = PARTS // 2
    bw = 2 * cols

    def part_cols(j):
        return slice(j * bw, (j + 1) * bw)

    for j in range(blocks):
        unpack(0, 2 * j)
        unpack(0, 2 * j + 1)

        def tokens_pre(g, carry, j=j):
            pre[g, :, part_cols(j)] = jnp.maximum(
                jnp.dot(tok[0, g], wn[0, :, part_cols(j)], preferred_element_type=jnp.float32), 0.0
            )
            return carry

        lax.fori_loop(0, 4, tokens_pre, 0)

    for q in range(pieces):
        forward(1, q)
    for j in range(blocks):
        unpack(1, 2 * j)
        unpack(1, 2 * j + 1)
    for q in range(pieces):
        forward_copy(1, q).wait_recv()
    transpose(1, 2)
    transpose(1, 3)

    offset = (0, 16, 24, 28, 30)
    half = (16, 8, 4, 2, 1)

    def reduce_copy(r, k):
        return remote(
            gbuf.at[r, pl.ds(half[k], half[k])],
            rbuf.at[r, pl.ds(offset[k], half[k])],
            r_s.at[r, k],
            r_r.at[r, k],
            near[ORDERS[r % PARTS][STEPS - 1 - k]],
        )

    def reduce_step(r, k):
        reduce_copy(r, k).wait_recv()
        h, o = half[k], offset[k]
        if k < STEPS - 1:
            n = h // 2
            gbuf[r, n:h] = gbuf[r, n:h] + rbuf[r, o + n : o + h]
            start(reduce_copy(r, k + 1))
            gbuf[r, 0:n] = gbuf[r, 0:n] + rbuf[r, o : o + n]

    def weight_grad(m, j, right):
        per = width // 4 // shard

        def some(i, carry):
            out = jnp.dot(
                tokt[m, pl.ds(pl.multiple_of(i * (width // 4), width // 4), width // 4), :],
                right(),
                preferred_element_type=jnp.float32,
            )
            for t in range(per):
                rel = relative(i * per + t)
                for e in range(2):
                    p = 2 * j + e
                    gbuf[(1 - m) * PARTS + p, slot(rel, p)] = out[
                        t * shard : (t + 1) * shard, e * cols : (e + 1) * cols
                    ]
            return carry

        lax.fori_loop(0, 4, some, 0)

    total = 4 * rows
    for j in range(blocks):

        def activate(g, carry, j=j):
            kept = pre[g, :, part_cols(j)]
            act[pl.ds(pl.multiple_of(g * rows, rows), rows), :] = (kept * kept).astype(jnp.bfloat16)
            return carry

        lax.fori_loop(0, 4, activate, 0)
        weight_grad(1, j, lambda: act[...])
        start(reduce_copy(2 * j, 0))
        start(reduce_copy(2 * j + 1, 0))

    for j in range(blocks):

        def back(g, carry, j=j):
            value = jnp.dot(tok[1, g], wn[1, :, part_cols(j)], preferred_element_type=jnp.float32)
            gpre[pl.ds(pl.multiple_of(g * rows, rows), rows), part_cols(j)] = (
                2.0 * pre[g, :, part_cols(j)] * value
            ).astype(jnp.bfloat16)
            return carry

        lax.fori_loop(0, 4, back, 0)
        weight_grad(0, j, lambda j=j: gpre[:, part_cols(j)])
        start(reduce_copy(PARTS + 2 * j, 0))
        start(reduce_copy(PARTS + 2 * j + 1, 0))
        reduce_step(2 * j, 0)
        reduce_step(2 * j + 1, 0)

    def inputs_grad(n, carry):
        columns = pl.ds(pl.multiple_of(n * bw, bw), bw)
        w = wn[0, pl.ds(pl.multiple_of(n * bw, bw), bw), :]
        for g in range(4):
            pre[g, :, columns] = contract(gpre[g * rows : (g + 1) * rows, :], w, 1, 1)
        return carry

    lax.fori_loop(0, width // bw, inputs_grad, 0)

    def share_copy(i):
        return remote(pre.at[1 + 2 * i], part_in.at[i], pi_s.at[i], pi_r.at[i], sibling)

    def pair_copy(q):
        return remote(
            pair_in.at[0, pl.ds(q * chunk, chunk)],
            pair_in.at[1, pl.ds(q * chunk, chunk)],
            li_s.at[q],
            li_r.at[q],
            pair,
        )

    start(share_copy(1))
    start(share_copy(0))
    for p in range(PARTS):
        reduce_step(p, 1)
    share_copy(1).wait_recv()
    for q in range(pieces):
        s = slice(q * chunk, (q + 1) * chunk)
        pair_in[0, s] = pre[2, s] + part_in[1, s]
        start(pair_copy(q))
    share_copy(0).wait_recv()
    pre[0] = pre[0] + part_in[0]
    for p in range(PARTS):
        reduce_step(PARTS + p, 0)
    for p in range(PARTS):
        reduce_step(p, 2)
    for p in range(PARTS):
        reduce_step(PARTS + p, 1)
    for p in range(PARTS):
        reduce_step(p, 3)

    def twin_copy(r):
        place = outs.at[r // PARTS, :, pl.ds(pl.multiple_of(base + (r % PARTS) * cols, cols), cols)]
        return remote(place, place, rep_s.at[r], rep_r.at[r], twin)

    def finish(r):
        reduce_step(r, STEPS - 1)
        value = (gbuf[r, 0] + rbuf[r, 30]) * factor
        outs[r // PARTS, :, pl.ds(pl.multiple_of(base + (r % PARTS) * cols, cols), cols)] = value
        start(twin_copy(r))
        return value

    for p in range(PARTS):
        value = finish(p)
        ebuf[0, p : p + 1, :] = jnp.sum(value * value, axis=0, keepdims=True)

    def energy_copy(k):
        if k < STEPS:
            return remote(ebuf.at[k], esum.at[k], e_s.at[k], e_r.at[k], near[k])
        return remote(ebuf.at[k], esum.at[k], e_s.at[k], e_r.at[k], twin)

    def energy_step(k):
        energy_copy(k).wait_recv()
        ebuf[k + 1] = ebuf[k] + esum[k]
        start(energy_copy(k + 1))

    start(energy_copy(0))
    for p in range(PARTS):
        reduce_step(PARTS + p, 2)
    energy_step(0)
    for p in range(PARTS):
        reduce_step(PARTS + p, 3)
    energy_step(1)
    for p in range(PARTS):
        finish(PARTS + p)
    energy_step(2)
    energy_step(3)
    energy_step(4)
    for q in range(pieces):
        pair_copy(q).wait_recv()
    gin_ref[...] = (pre[0] + pair_in[1]).astype(jnp.bfloat16)
    for p in range(PARTS):
        twin_copy(p).wait_recv()
    gdn_ref[...] = outs[0]
    for p in range(PARTS):
        twin_copy(PARTS + p).wait_recv()
    gup = outs[1]
    gup_ref[...] = gup
    own = jnp.sum(gup * gup, axis=1, keepdims=True)
    eup_own[...] = jnp.broadcast_to(own, eup_own.shape)
    up_copy = remote(eup_own, eup_in, eu_s, eu_r, sibling)
    start(up_copy)
    energy_copy(STEPS).wait_recv()
    edn_ref[rep] = ebuf[STEPS] * (1.0 / width)
    edn_ref[1 - rep] = esum[STEPS] * (1.0 / width)
    up_copy.wait_recv()
    eup_ref[...] = (eup_own[...] + eup_in[...]) * (1.0 / (hidden * 4))
    for copy in pending:
        copy.wait_send()


def body(inputs, up_proj, down_proj, out_cotangent):
    rows, width = inputs.shape
    shard, both = up_proj.shape
    hidden = both // 2
    cols = hidden // PARTS
    factor = float(rows * lax.axis_size("rep") * lax.axis_size("fs") * lax.axis_size("tp")) ** (-0.5)
    f32, bf16 = jnp.float32, jnp.bfloat16
    shape = jax.ShapeDtypeStruct
    vmem = pl.BlockSpec(memory_space=pltpu.VMEM)
    dma = pltpu.SemaphoreType.DMA
    gin, gup, gdn, eup, edn = pl.pallas_call(
        functools.partial(kernel, factor),
        out_shape=(
            shape((rows, width), bf16),
            shape((shard, both), f32),
            shape((shard, both), f32),
            shape((shard, 128), f32),
            shape((2, PARTS, cols), f32),
        ),
        in_specs=[vmem] * 4,
        out_specs=(vmem,) * 5,
        scratch_shapes=[
            pltpu.VMEM((2, 4, rows, width), bf16),
            pltpu.VMEM((2, width, 4 * rows), bf16),
            pltpu.VMEM((2, PARTS, 32, shard, cols), bf16),
            pltpu.VMEM((2, width, hidden), bf16),
            pltpu.VMEM((4, rows, max(hidden, width)), f32),
            pltpu.VMEM((4 * rows, 2 * cols), bf16),
            pltpu.VMEM((4 * rows, hidden), bf16),
            pltpu.VMEM((2 * PARTS, 32, shard, cols), f32),
            pltpu.VMEM((2 * PARTS, 31, shard, cols), f32),
            pltpu.VMEM((2, rows, width), f32),
            pltpu.VMEM((2, rows, width), f32),
            pltpu.VMEM((8, 128), f32),
            pltpu.VMEM((2, shard, both), f32),
            pltpu.VMEM((STEPS + 1, PARTS, cols), f32),
            pltpu.VMEM((STEPS + 1, PARTS, cols), f32),
            pltpu.VMEM((shard, 128), f32),
            pltpu.VMEM((shard, 128), f32),
            dma((2, 2)),
            dma((2, 2)),
            dma((2, 2)),
            dma((2, 2)),
            dma((2,)),
            dma((2,)),
            dma((2 * PARTS, STEPS)),
            dma((2 * PARTS, STEPS)),
            dma((2 * PARTS, STEPS)),
            dma((2 * PARTS, STEPS)),
            dma((2 * PARTS,)),
            dma((2 * PARTS,)),
            dma((2,)),
            dma((2,)),
            dma((2,)),
            dma((2,)),
            dma((STEPS + 1,)),
            dma((STEPS + 1,)),
            dma,
            dma,
        ],
        compiler_params=pltpu.CompilerParams(
            collective_id=0, has_side_effects=True, vmem_limit_bytes=60 * 2**20
        ),
        name="step",
    )(inputs, out_cotangent, up_proj, down_proj.T)
    return gin, gup, gdn.T, eup[:, 0], edn.reshape((both,))


def solution(mesh):
    return jax.shard_map(
        body,
        mesh=mesh,
        in_specs=(
            P(("rep", "fs", "tp"), None),
            P("fs", "tp"),
            P("tp", "fs"),
            P(("rep", "fs", "tp"), None),
        ),
        out_specs=(P(("rep", "fs", "tp"), None), P("fs", "tp"), P("tp", "fs"), P("fs"), P("tp")),
        check_vma=False,
    )
```

profile of v0, /device:TPU:0, one launch (start us, length us, event | category | flops | bytes accessed | tf_op | source)
XLA Modules:
  0.0 141.7 jit_solution(9454060572103931084)
XLA Ops:
  0.6 135.5 %step.1 = (bf16[256,1024]{1,0:T(8,128)(2,1)}, f32[32,2048]{1,0:T(8,128)}, f32[32,2048]{1,0:T(8,128)}, f32[32,128]{1,0:T(8,128)}, f32[2,8,128]{2,1,0:T(8,128)}) custom-call(bf16[256,1024]{1,0:T(8,128)(2,1)} %x_ref.1, bf16[256,1024]{1,0:T(8,128)(2,1)} %c_ref.1, bf16[32,2048]{1,0:T(8,128)(2,1)} %u_ref.1, bf16[32,2048]{1,0:T(8,128)(2,1)} %bitcast.4), custom_call_target="tpu_custom_call" | custom-call | tf_op jit(solution)/shard_map/step/pallas_call | solution.py:436
  136.1 1.3 slice_reduce_fusion
  137.4 0.0 copy-start.1
  137.4 1.9 %copy.13 = bf16[256,1024]{1,0:T(8,128)(2,1)} copy(bf16[256,1024]{1,0:T(8,128)(2,1)} %get-tuple-element.20) | data formatting | bytes 1048576
  139.4 0.0 copy-done.1
  139.4 0.0 copy-start
  139.4 0.7 copy.14
  140.1 0.3 copy-done
  140.4 0.0 copy-start.2
  140.4 0.7 copy.15
  141.1 0.0 copy-done.2
  141.1 0.6 copy.16
Async XLA Ops:
  137.4 1.9 %copy-start.1 = (f32[32,2048]{1,0:T(8,128)S(1)}, f32[32,2048]{1,0:T(8,128)}, u32[]{:S(2)}) copy-start(f32[32,2048]{1,0:T(8,128)} %get-tuple-element.21) | copy-start | bytes 786436
  139.4 1.0 copy-start
  140.4 0.7 copy-start.2
where the time goes:
time: 142 us
  Pallas kernels  135 us (95%)
  local copies, waits for them, and re-layouts  5.61 us (4%)
    pallas_call x1, Pallas kernels, body(): pl.pallas_call(functools.partial(kernel, factor), out_shape=(shape((rows,...  135 us
    unnamed x10, local copies, waits for them, and re-layouts  4.26 us

commit v1 on v0

--- a/solution.py
+++ b/solution.py
@@ -19,6 +19,7 @@
     (3, 2, 1, 4, 0),
 )
 STEPS = 5
+SPLIT = 2
 PARTS = len(ORDERS)
 
 
@@ -72,7 +73,6 @@
     rbuf,
     part_in,
     pair_in,
-    last_in,
     outs,
     ebuf,
     esum,
@@ -120,7 +120,7 @@
         pl.semaphore_signal(barrier, inc=1, device_id=device, device_id_type=MESH)
 
     for m in range(2):
-        tok[m, 0] = tokens[m][...]
+        tok[m, 0:rows] = tokens[m][...]
         for p in range(PARTS):
             wg[m, p, 0] = weights[m][:, pl.ds(pl.multiple_of(base + p * cols, cols), cols)]
 
@@ -136,7 +136,7 @@
     def token_copy(m, q):
         return remote(
             tokens[m].at[pl.ds(q * chunk, chunk)],
-            tok.at[m, 2, pl.ds(q * chunk, chunk)],
+            tok.at[m, pl.ds(2 * rows + q * chunk, chunk)],
             tok_s.at[m, q],
             tok_r.at[m, q],
             pair,
@@ -144,15 +144,15 @@
 
     def forward_copy(m, q):
         return remote(
-            tok.at[m, 2, pl.ds(q * chunk, chunk)],
-            tok.at[m, 3, pl.ds(q * chunk, chunk)],
+            tok.at[m, pl.ds(2 * rows + q * chunk, chunk)],
+            tok.at[m, pl.ds(3 * rows + q * chunk, chunk)],
             fwd_s.at[m, q],
             fwd_r.at[m, q],
             sibling,
         )
 
     def sibling_copy(m):
-        return remote(tokens[m], tok.at[m, 1], sib_s.at[m], sib_r.at[m], sibling)
+        return remote(tokens[m], tok.at[m, pl.ds(rows, rows)], sib_s.at[m], sib_r.at[m], sibling)
 
     def gather_copy(m, p, k):
         if k == 0:
@@ -181,7 +181,7 @@
         start(sibling_copy(m))
 
     def transpose(m, g):
-        tokt[m, :, g * rows : (g + 1) * rows] = tok[m, g].T
+        tokt[m, :, g * rows : (g + 1) * rows] = tok[m, g * rows : (g + 1) * rows].T
 
     gather_step(0, 1)
     gather_step(1, 1)
@@ -198,27 +198,28 @@
     gather_step(0, 4)
     gather_step(1, 4)
 
-    def slot(bits, p):
-        total = 0
-        for k in range(STEPS):
-            total = total + bits[ORDERS[p][k]] * 2**k
-        return total
-
-    def relative(shard_index):
-        return [(a + b) % 2 for a, b in zip(mine, bits_of(shard_index))]
+    flip = [(bit, 1 - bit) for bit in mine]
+    tables = {}
+
+    def slot(s, p):
+        order = ORDERS[p]
+        if order not in tables:
+            place = {d: 2**k for k, d in enumerate(order)}
+            high, low = [], []
+            for v in range(8):
+                bits = bits_of(4 * v)
+                high.append(sum(flip[d][bits[d]] * place[d] for d in (0, 1, 2)))
+            for v in range(4):
+                bits = bits_of(v)
+                low.append(sum(flip[d][bits[d]] * place[d] for d in (3, 4)))
+            tables[order] = high, low
+        high, low = tables[order]
+        return high[s // 4] + low[s % 4]
 
     def unpack(m, p):
         gather_copy(m, p, STEPS - 1).wait_recv()
-
-        def some(i, carry):
-            for t in range(8):
-                s = i * 8 + t
-                wn[m, pl.ds(pl.multiple_of(s * shard, shard), shard), p * cols : (p + 1) * cols] = wg[
-                    m, p, slot(relative(s), p)
-                ]
-            return carry
-
-        lax.fori_loop(0, 4, some, 0)
+        for s in range(32):
+            wn[m, s * shard : (s + 1) * shard, p * cols : (p + 1) * cols] = wg[m, p, slot(s, p)]
 
     for q in range(pieces):
         forward_copy(0, q).wait_recv()
@@ -226,6 +227,8 @@
     transpose(0, 3)
     blocks = PARTS // 2
     bw = 2 * cols
+    total = 4 * rows
+    big = total // SPLIT
 
     def part_cols(j):
         return slice(j * bw, (j + 1) * bw)
@@ -234,13 +237,15 @@
         unpack(0, 2 * j)
         unpack(0, 2 * j + 1)
 
-        def tokens_pre(g, carry, j=j):
-            pre[g, :, part_cols(j)] = jnp.maximum(
-                jnp.dot(tok[0, g], wn[0, :, part_cols(j)], preferred_element_type=jnp.float32), 0.0
+        for i in range(total // big):
+            pre[i * big : (i + 1) * big, part_cols(j)] = jnp.maximum(
+                jnp.dot(
+                    tok[0, i * big : (i + 1) * big],
+                    wn[0, :, part_cols(j)],
+                    preferred_element_type=jnp.float32,
+                ),
+                0.0,
             )
-            return carry
-
-        lax.fori_loop(0, 4, tokens_pre, 0)
 
     for q in range(pieces):
         forward(1, q)
@@ -274,65 +279,45 @@
             gbuf[r, 0:n] = gbuf[r, 0:n] + rbuf[r, o : o + n]
 
     def weight_grad(m, j, right):
-        per = width // 4 // shard
-
-        def some(i, carry):
+        tall = width // SPLIT
+        per = tall // shard
+        for i in range(SPLIT):
             out = jnp.dot(
-                tokt[m, pl.ds(pl.multiple_of(i * (width // 4), width // 4), width // 4), :],
-                right(),
-                preferred_element_type=jnp.float32,
+                tokt[m, i * tall : (i + 1) * tall, :], right(), preferred_element_type=jnp.float32
             )
             for t in range(per):
-                rel = relative(i * per + t)
                 for e in range(2):
                     p = 2 * j + e
-                    gbuf[(1 - m) * PARTS + p, slot(rel, p)] = out[
+                    gbuf[(1 - m) * PARTS + p, slot(i * per + t, p)] = out[
                         t * shard : (t + 1) * shard, e * cols : (e + 1) * cols
                     ]
-            return carry
-
-        lax.fori_loop(0, 4, some, 0)
-
-    total = 4 * rows
+
     for j in range(blocks):
-
-        def activate(g, carry, j=j):
-            kept = pre[g, :, part_cols(j)]
-            act[pl.ds(pl.multiple_of(g * rows, rows), rows), :] = (kept * kept).astype(jnp.bfloat16)
-            return carry
-
-        lax.fori_loop(0, 4, activate, 0)
+        kept = pre[:, part_cols(j)]
+        act[...] = (kept * kept).astype(jnp.bfloat16)
         weight_grad(1, j, lambda: act[...])
         start(reduce_copy(2 * j, 0))
         start(reduce_copy(2 * j + 1, 0))
 
     for j in range(blocks):
-
-        def back(g, carry, j=j):
-            value = jnp.dot(tok[1, g], wn[1, :, part_cols(j)], preferred_element_type=jnp.float32)
-            gpre[pl.ds(pl.multiple_of(g * rows, rows), rows), part_cols(j)] = (
-                2.0 * pre[g, :, part_cols(j)] * value
-            ).astype(jnp.bfloat16)
-            return carry
-
-        lax.fori_loop(0, 4, back, 0)
+        for i in range(SPLIT):
+            part = slice(i * big, (i + 1) * big)
+            value = jnp.dot(tok[1, part], wn[1, :, part_cols(j)], preferred_element_type=jnp.float32)
+            gpre[part, part_cols(j)] = (2.0 * pre[part, part_cols(j)] * value).astype(jnp.bfloat16)
         weight_grad(0, j, lambda j=j: gpre[:, part_cols(j)])
         start(reduce_copy(PARTS + 2 * j, 0))
         start(reduce_copy(PARTS + 2 * j + 1, 0))
         reduce_step(2 * j, 0)
         reduce_step(2 * j + 1, 0)
 
-    def inputs_grad(n, carry):
-        columns = pl.ds(pl.multiple_of(n * bw, bw), bw)
-        w = wn[0, pl.ds(pl.multiple_of(n * bw, bw), bw), :]
-        for g in range(4):
-            pre[g, :, columns] = contract(gpre[g * rows : (g + 1) * rows, :], w, 1, 1)
-        return carry
-
-    lax.fori_loop(0, width // bw, inputs_grad, 0)
+    for n in range(width // bw):
+        w = wn[0, n * bw : (n + 1) * bw, :]
+        for i in range(SPLIT):
+            part = slice(i * big, (i + 1) * big)
+            pre[part, n * bw : (n + 1) * bw] = contract(gpre[part, :], w, 1, 1)
 
     def share_copy(i):
-        return remote(pre.at[1 + 2 * i], part_in.at[i], pi_s.at[i], pi_r.at[i], sibling)
+        return remote(pre.at[pl.ds((1 + 2 * i) * rows, rows)], part_in.at[i], pi_s.at[i], pi_r.at[i], sibling)
 
     def pair_copy(q):
         return remote(
@@ -350,10 +335,10 @@
     share_copy(1).wait_recv()
     for q in range(pieces):
         s = slice(q * chunk, (q + 1) * chunk)
-        pair_in[0, s] = pre[2, s] + part_in[1, s]
+        pair_in[0, s] = pre[2 * rows + q * chunk : 2 * rows + (q + 1) * chunk] + part_in[1, s]
         start(pair_copy(q))
     share_copy(0).wait_recv()
-    pre[0] = pre[0] + part_in[0]
+    pre[0:rows] = pre[0:rows] + part_in[0]
     for p in range(PARTS):
         reduce_step(PARTS + p, 0)
     for p in range(PARTS):
@@ -402,7 +387,7 @@
     energy_step(4)
     for q in range(pieces):
         pair_copy(q).wait_recv()
-    gin_ref[...] = (pre[0] + pair_in[1]).astype(jnp.bfloat16)
+    gin_ref[...] = (pre[0:rows] + pair_in[1]).astype(jnp.bfloat16)
     for p in range(PARTS):
         twin_copy(p).wait_recv()
     gdn_ref[...] = outs[0]
@@ -445,18 +430,17 @@
         in_specs=[vmem] * 4,
         out_specs=(vmem,) * 5,
         scratch_shapes=[
-            pltpu.VMEM((2, 4, rows, width), bf16),
+            pltpu.VMEM((2, 4 * rows, width), bf16),
             pltpu.VMEM((2, width, 4 * rows), bf16),
             pltpu.VMEM((2, PARTS, 32, shard, cols), bf16),
             pltpu.VMEM((2, width, hidden), bf16),
-            pltpu.VMEM((4, rows, max(hidden, width)), f32),
+            pltpu.VMEM((4 * rows, max(hidden, width)), f32),
             pltpu.VMEM((4 * rows, 2 * cols), bf16),
             pltpu.VMEM((4 * rows, hidden), bf16),
             pltpu.VMEM((2 * PARTS, 32, shard, cols), f32),
             pltpu.VMEM((2 * PARTS, 31, shard, cols), f32),
             pltpu.VMEM((2, rows, width), f32),
             pltpu.VMEM((2, rows, width), f32),
-            pltpu.VMEM((8, 128), f32),
             pltpu.VMEM((2, shard, both), f32),
             pltpu.VMEM((STEPS + 1, PARTS, cols), f32),
             pltpu.VMEM((STEPS + 1, PARTS, cols), f32),

time: 142 us -> 117 us (0.82)
  Pallas kernels: 135 us -> 111 us
    pallas_call x1, Pallas kernels: 135 us -> 111 us  [body(): pl.pallas_call(functools.partial(kernel, factor), out_shape=(shape((rows,...]
where the time goes in v1:
time: 117 us
  Pallas kernels  111 us (95%)
  local copies, waits for them, and re-layouts  5.61 us (5%)
    pallas_call x1, Pallas kernels, body(): pl.pallas_call(functools.partial(kernel, factor), out_shape=(shape((rows,...  111 us
    unnamed x10, local copies, waits for them, and re-layouts  4.26 us

profile of v1, /device:TPU:0, one launch (start us, length us, event | category | flops | bytes accessed | tf_op | source)
XLA Modules:
  0.0 117.2 jit_solution(1607924561885359168)
XLA Ops:
  0.6 110.9 %step.1 = (bf16[256,1024]{1,0:T(8,128)(2,1)}, f32[32,2048]{1,0:T(8,128)}, f32[32,2048]{1,0:T(8,128)}, f32[32,128]{1,0:T(8,128)}, f32[2,8,128]{2,1,0:T(8,128)}) custom-call(bf16[256,1024]{1,0:T(8,128)(2,1)} %x_ref.1, bf16[256,1024]{1,0:T(8,128)(2,1)} %c_ref.1, bf16[32,2048]{1,0:T(8,128)(2,1)} %u_ref.1, bf16[32,2048]{1,0:T(8,128)(2,1)} %bitcast.4), custom_call_target="tpu_custom_call" | custom-call | tf_op jit(solution)/shard_map/step/pallas_call | solution.py:421
  111.6 1.3 %slice_reduce_fusion = f32[32]{0:T(128)} fusion(f32[32,128]{1,0:T(8,128)} %get-tuple-element.13), kind=kLoop, calls=%fused_computation | loop fusion | bytes 256 | tf_op jit(solution)/shard_map/slice | solution.py:475
  112.9 0.0 copy-start.1
  112.9 1.9 %copy.13 = bf16[256,1024]{1,0:T(8,128)(2,1)} copy(bf16[256,1024]{1,0:T(8,128)(2,1)} %get-tuple-element.20) | data formatting | bytes 1048576
  114.8 0.0 copy-done.1
  114.8 0.0 copy-start
  114.8 0.7 copy.14
  115.5 0.3 copy-done
  115.9 0.0 copy-start.2
  115.9 0.7 copy.15
  116.6 0.0 copy-done.2
  116.6 0.6 copy.16
Async XLA Ops:
  112.9 1.9 %copy-start.1 = (f32[32,2048]{1,0:T(8,128)S(1)}, f32[32,2048]{1,0:T(8,128)}, u32[]{:S(2)}) copy-start(f32[32,2048]{1,0:T(8,128)} %get-tuple-element.21) | copy-start | bytes 786436
  114.8 1.0 copy-start
  115.9 0.7 copy-start.2

commit v2 on v1

v2 whole, which is shorter than its diff:
```python
import functools

import jax
import jax.numpy as jnp
from jax import lax
from jax.experimental import pallas as pl
from jax.experimental.pallas import tpu as pltpu
from jax.sharding import PartitionSpec as P

MESH = pl.DeviceIdType.MESH
SIZES = ((3, 3, 3, 3, 4), (4, 3, 3, 3, 3))
STARTS = tuple(tuple(sum(size[:i]) for i in range(5)) for size in SIZES)
STEPS = 5
PARTS = 5
SPLIT = 2
ORDERS = tuple(tuple((i + 1 + k) % 5 for k in range(STEPS)) for i in range(PARTS))
UNITS = 16
BLOCKS = 8
HALF = (16, 8, 4, 2, 1)
SPAN = 240.0
SHIFT = 120.0


def encode(value, scale):
    code = jnp.exp2(jnp.abs(value) * (SPAN / scale) - SHIFT)
    return jnp.where(value < 0.0, -code, code).astype(jnp.bfloat16)


def decode(code, scale):
    code = code.astype(jnp.float32)
    size = (jnp.log2(jnp.abs(code)) + SHIFT) * (scale * (1.0 / SPAN))
    return jnp.where(code < 0.0, -size, size)


def scale_of(top):
    return (top * 1.01 + 1e-35).astype(jnp.bfloat16)


def bits_of(fs):
    z, y, x = fs // 16, (fs // 4) % 4, fs % 4
    return (z, (y % 2 + y // 2) % 2, y // 2, (x % 2 + x // 2) % 2, x // 2)


def partners_of(fs):
    z, y, x = fs // 16, (fs // 4) % 4, fs % 4
    return (
        fs + 16 - 32 * z,
        fs + 4 - 8 * (y % 2),
        fs + 12 - 8 * y,
        fs + 1 - 2 * (x % 2),
        fs + 3 - 2 * x,
    )


def remote(src, dst, send, recv, device):
    return pltpu.make_async_remote_copy(
        src_ref=src, dst_ref=dst, send_sem=send, recv_sem=recv, device_id=device, device_id_type=MESH
    )


def contract(left, right, left_dim, right_dim):
    return lax.dot_general(
        left, right, (((left_dim,), (right_dim,)), ((), ())), preferred_element_type=jnp.float32
    )


def kernel(
    factor,
    x_ref,
    c_ref,
    u_ref,
    d_ref,
    gin_ref,
    gup_ref,
    gdn_ref,
    eup_ref,
    edn_ref,
    tok,
    tokt,
    wg,
    wn,
    pre,
    act,
    gpre,
    gbuf,
    sbuf,
    rbuf,
    part_in,
    pair_out,
    pair_in,
    outs,
    ebuf,
    esum,
    eup_own,
    eup_in,
    tok_s,
    tok_r,
    fwd_s,
    fwd_r,
    sib_s,
    sib_r,
    g_s,
    g_r,
    r_s,
    r_r,
    rep_s,
    rep_r,
    pi_s,
    pi_r,
    li_s,
    li_r,
    e_s,
    e_r,
    eu_s,
    eu_r,
):
    rep, fs, tp = lax.axis_index("rep"), lax.axis_index("fs"), lax.axis_index("tp")
    mine = bits_of(fs)
    near = [{"fs": other} for other in partners_of(fs)]
    sibling = {"tp": 1 - tp}
    pair = {"rep": 1 - rep, "fs": partners_of(fs)[0]}
    twin = {"rep": 1 - rep}
    rows, width = x_ref.shape
    shard = u_ref.shape[0]
    hidden = u_ref.shape[1] // 2
    base = rep * hidden
    weights = (u_ref, d_ref)
    tokens = (x_ref, c_ref)
    pieces = 2
    chunk = rows // pieces
    half_rows = 2 * rows
    bw = 256
    blocks = hidden // bw
    all_parts = range(PARTS)
    f32, bf16 = jnp.float32, jnp.bfloat16

    flip = [(bit, 1 - bit) for bit in mine]
    tables = {}

    def unit(m, s, u):
        p = max(i for i in all_parts if STARTS[m][i] <= u)
        size = SIZES[m][p]
        if (p, size) not in tables:
            place = {d: size * 2**k for k, d in enumerate(ORDERS[p])}
            high, low = [], []
            for v in range(8):
                bits = bits_of(4 * v)
                high.append(sum(flip[d][bits[d]] * place[d] for d in (0, 1, 2)))
            for v in range(4):
                bits = bits_of(v)
                low.append(sum(flip[d][bits[d]] * place[d] for d in (3, 4)))
            tables[p, size] = high, low
        high, low = tables[p, size]
        return high[s // 4] + low[s % 4] + (m * UNITS * 32 + STARTS[m][p] * 32 + u - STARTS[m][p])

    def home(m, p):
        return m * UNITS * 32 + STARTS[m][p] * 32

    barrier = pltpu.get_barrier_semaphore()
    for device in near + [sibling, pair, twin]:
        pl.semaphore_signal(barrier, inc=1, device_id=device, device_id_type=MESH)

    for m in range(2):
        tok[m, 0:rows] = tokens[m][...]
        for p in all_parts:
            for i in range(SIZES[m][p]):
                block, row = divmod(STARTS[m][p] + i, 2)
                wg[home(m, p) + i] = weights[m][
                    row * 16 : row * 16 + 16, pl.ds(pl.multiple_of(base + block * 128, 128), 128)
                ]

    pl.semaphore_wait(barrier, STEPS + 3)

    pending = []

    def start(copy):
        copy.start()
        pending.append(copy)
        return copy

    def token_copy(m, q):
        return remote(
            tokens[m].at[pl.ds(q * chunk, chunk)],
            tok.at[m, pl.ds(2 * rows + q * chunk, chunk)],
            tok_s.at[m, q],
            tok_r.at[m, q],
            pair,
        )

    def forward_copy(m, q):
        return remote(
            tok.at[m, pl.ds(2 * rows + q * chunk, chunk)],
            tok.at[m, pl.ds(3 * rows + q * chunk, chunk)],
            fwd_s.at[m, q],
            fwd_r.at[m, q],
            sibling,
        )

    def sibling_copy(m):
        return remote(tokens[m], tok.at[m, pl.ds(rows, rows)], sib_s.at[m], sib_r.at[m], sibling)

    def gather_copy(m, p, k):
        n = SIZES[m][p] * 2**k
        return remote(
            wg.at[pl.ds(home(m, p), n)],
            wg.at[pl.ds(home(m, p) + n, n)],
            g_s.at[m, p, k],
            g_r.at[m, p, k],
            near[ORDERS[p][k]],
        )

    def gather_step(m, k):
        for p in all_parts:
            if k > 0:
                gather_copy(m, p, k - 1).wait_recv()
            start(gather_copy(m, p, k))

    def forward(m, q):
        token_copy(m, q).wait_recv()
        start(forward_copy(m, q))

    def transpose(m, g):
        tokt[m, :, g * rows : (g + 1) * rows] = tok[m, g * rows : (g + 1) * rows].T

    def unpack(m):
        for p in all_parts:
            gather_copy(m, p, STEPS - 1).wait_recv()
            for u in range(STARTS[m][p], STARTS[m][p] + SIZES[m][p]):
                block, row = divmod(u, 2)
                for s in range(32):
                    top = s * shard + row * 16
                    wn[m, top : top + 16, block * 128 : block * 128 + 128] = wg[unit(m, s, u)]

    def part_cols(j):
        return slice(j * bw, (j + 1) * bw)

    def forward_half(h):
        part = slice(h * half_rows, (h + 1) * half_rows)
        for j in range(blocks):
            kept = jnp.maximum(
                jnp.dot(tok[0, part], wn[0, :, part_cols(j)], preferred_element_type=f32), 0.0
            )
            pre[part, part_cols(j)] = kept
            act[part, part_cols(j)] = (kept * kept).astype(bf16)

    def back_half(h):
        part = slice(h * half_rows, (h + 1) * half_rows)
        for j in range(blocks):
            value = jnp.dot(tok[1, part], wn[1, :, part_cols(j)], preferred_element_type=f32)
            gpre[part, part_cols(j)] = (2.0 * pre[part, part_cols(j)] * value).astype(bf16)

    def room(m, p, k):
        before = sum(1 + HALF[i] * SIZES[m][p] for i in range(k))
        return m * (31 * UNITS + 25) + 31 * STARTS[m][p] + 5 * p + before

    def reduce_copy(m, p, k):
        n = 1 + HALF[k] * SIZES[m][p]
        place = pl.ds(room(m, p, k), n)
        return remote(
            sbuf.at[place], rbuf.at[place], r_s.at[m, p, k], r_r.at[m, p, k], near[ORDERS[p][STEPS - 1 - k]]
        )

    def chunks(count, size):
        step = min(count, 4) * size
        return count * size // step, step

    def highest(m, p, k):
        n = SIZES[m][p]
        loops, step = chunks(HALF[k], n)
        at = home(m, p) + HALF[k] * n

        def some(i, top):
            return jnp.maximum(top, jnp.max(jnp.abs(gbuf[pl.ds(at + i * step, step)]), axis=0))

        return lax.fori_loop(0, loops, some, jnp.zeros((16, 128), f32))

    def send_sums(m, p, k, top):
        n = SIZES[m][p]
        loops, step = chunks(HALF[k], n)
        at, to = home(m, p) + HALF[k] * n, room(m, p, k)
        coded = scale_of(top)
        sbuf[to] = coded
        scale = coded.astype(f32)

        def some(i, carry):
            sbuf[pl.ds(to + 1 + i * step, step)] = encode(gbuf[pl.ds(at + i * step, step)], scale)
            return carry

        lax.fori_loop(0, loops, some, 0)
        start(reduce_copy(m, p, k))

    def begin(m, p):
        send_sums(m, p, 0, highest(m, p, 0))

    def add_sums(m, p, k, first, count):
        n = SIZES[m][p]
        loops, step = chunks(count, n)
        at, got = home(m, p) + first * n, room(m, p, k) + 1 + first * n
        scale = rbuf[room(m, p, k)].astype(f32)

        def some(i, top):
            place = pl.ds(at + i * step, step)
            value = gbuf[place] + decode(rbuf[pl.ds(got + i * step, step)], scale)
            gbuf[place] = value
            return jnp.maximum(top, jnp.max(jnp.abs(value), axis=0))

        return lax.fori_loop(0, loops, some, jnp.zeros((16, 128), f32))

    def reduce_step(m, k):
        for p in all_parts:
            reduce_copy(m, p, k).wait_recv()
            n = HALF[k + 1]
            top = add_sums(m, p, k, n, n)
            send_sums(m, p, k + 1, top)
            add_sums(m, p, k, 0, n)

    def weight_grad(m, right):
        tall = width // SPLIT
        done = 0
        for j in range(blocks):
            for i in range(SPLIT):
                out = jnp.dot(
                    tokt[m, i * tall : (i + 1) * tall, :], right[:, part_cols(j)], preferred_element_type=f32
                )
                for t in range(tall // shard):
                    for u in range(4):
                        block, row = divmod(u, 2)
                        gbuf[unit(m, i * (tall // shard) + t, 4 * j + u)] = out[
                            t * shard + row * 16 : t * shard + row * 16 + 16, block * 128 : block * 128 + 128
                        ]
            while done < PARTS and STARTS[m][done] + SIZES[m][done] <= 4 * (j + 1):
                begin(m, done)
                done += 1

    def share_copy(i):
        return remote(
            pre.at[pl.ds((1 + 2 * i) * rows, rows)], part_in.at[i], pi_s.at[i], pi_r.at[i], sibling
        )

    def pair_copy(q):
        return remote(pair_out.at[q], pair_in.at[q], li_s.at[q], li_r.at[q], pair)

    for m in range(2):
        gather_step(m, 0)
        for q in range(pieces):
            start(token_copy(m, q))
    for m in range(2):
        start(sibling_copy(m))
    for k in (1, 2):
        for m in range(2):
            gather_step(m, k)
    for m in range(2):
        transpose(m, 0)
        sibling_copy(m).wait_recv()
        transpose(m, 1)
    gather_step(0, 3)
    gather_step(1, 3)
    forward(0, 0)
    gather_step(0, 4)
    forward(0, 1)
    gather_step(1, 4)
    unpack(0)
    forward_half(0)
    for q in range(pieces):
        forward_copy(0, q).wait_recv()
    forward_half(1)
    transpose(0, 2)
    transpose(0, 3)
    unpack(1)
    forward(1, 0)
    back_half(0)
    forward(1, 1)
    transpose(1, 2)
    for q in range(pieces):
        forward_copy(1, q).wait_recv()
    transpose(1, 3)

    weight_grad(1, act)
    back_half(1)
    weight_grad(0, gpre)
    reduce_step(1, 0)

    for i in (1, 0):
        part = slice(i * half_rows, (i + 1) * half_rows)
        for n in range(width // bw):
            pre[part, n * bw : (n + 1) * bw] = contract(
                gpre[part, :], wn[0, n * bw : (n + 1) * bw, :], 1, 1
            )
        start(share_copy(i))

    reduce_step(0, 0)
    share_copy(1).wait_recv()
    for q in range(pieces):
        s = slice(q * chunk, (q + 1) * chunk)
        value = pre[2 * rows + q * chunk : 2 * rows + (q + 1) * chunk] + part_in[1, s]
        coded = scale_of(jnp.max(jnp.abs(value), axis=0, keepdims=True))
        pair_out[q, 0:16] = jnp.broadcast_to(coded, (16, width))
        pair_out[q, 16 : 16 + chunk] = encode(value, coded.astype(f32))
        start(pair_copy(q))
    share_copy(0).wait_recv()
    pre[0:rows] = pre[0:rows] + part_in[0]
    reduce_step(1, 1)
    reduce_step(0, 1)
    reduce_step(1, 2)
    reduce_step(0, 2)
    reduce_step(1, 3)

    def twin_copy(m, p):
        place = outs.at[m, rep, pl.ds(STARTS[m][p], SIZES[m][p])]
        return remote(place, place, rep_s.at[m, p], rep_r.at[m, p], twin)

    def finish(m, p):
        n = SIZES[m][p]
        reduce_copy(m, p, STEPS - 1).wait_recv()
        scale = rbuf[room(m, p, STEPS - 1)].astype(f32)
        got = decode(rbuf[pl.ds(room(m, p, STEPS - 1) + 1, n)], scale)
        value = (gbuf[pl.ds(home(m, p), n)] + got) * factor
        outs[m, rep, pl.ds(STARTS[m][p], n)] = value
        start(twin_copy(m, p))
        return value

    sums = []
    for p in all_parts:
        value = finish(1, p)
        for i in range(SIZES[1][p]):
            sums.append(jnp.sum(value[i] * value[i], axis=0, keepdims=True))
    for i in range(BLOCKS):
        ebuf[0, i : i + 1, :] = sums[2 * i] + sums[2 * i + 1]

    def energy_copy(k):
        device = near[k] if k < STEPS else twin
        return remote(ebuf.at[k], esum.at[k], e_s.at[k], e_r.at[k], device)

    def energy_step(k):
        energy_copy(k).wait_recv()
        ebuf[k + 1] = ebuf[k] + esum[k]
        start(energy_copy(k + 1))

    start(energy_copy(0))
    reduce_step(0, 3)
    energy_step(0)
    for p in all_parts:
        finish(0, p)
    energy_step(1)
    for q in range(pieces):
        pair_copy(q).wait_recv()
        s = slice(q * chunk, (q + 1) * chunk)
        scale = pair_in[q, 0:16].astype(f32)[0:1]
        gin_ref[s] = (pre[s] + decode(pair_in[q, 16 : 16 + chunk], scale)).astype(bf16)
    energy_step(2)

    def write(m, ref):
        for p in all_parts:
            twin_copy(m, p).wait_recv()
        for r in range(2):
            for u in range(UNITS):
                block, row = divmod(u, 2)
                left = r * hidden + block * 128
                ref[row * 16 : row * 16 + 16, left : left + 128] = outs[m, r, u]

    write(1, gdn_ref)
    energy_step(3)
    energy_step(4)
    write(0, gup_ref)
    for row in range(2):
        squares = jnp.zeros((16, 128), f32)
        for r in range(2):
            for block in range(BLOCKS):
                value = outs[0, r, 2 * block + row]
                squares = squares + value * value
        eup_own[row * 16 : row * 16 + 16, :] = jnp.broadcast_to(
            jnp.sum(squares, axis=1, keepdims=True), (16, 128)
        )
    up_copy = start(remote(eup_own, eup_in, eu_s, eu_r, sibling))
    energy_copy(STEPS).wait_recv()
    edn_ref[rep] = ebuf[STEPS] * (1.0 / width)
    edn_ref[1 - rep] = esum[STEPS] * (1.0 / width)
    up_copy.wait_recv()
    eup_ref[...] = (eup_own[...] + eup_in[...]) * (1.0 / (hidden * 4))
    for copy in pending:
        copy.wait_send()


def body(inputs, up_proj, down_proj, out_cotangent):
    rows, width = inputs.shape
    shard, both = up_proj.shape
    hidden = both // 2
    factor = float(rows * lax.axis_size("rep") * lax.axis_size("fs") * lax.axis_size("tp")) ** (-0.5)
    f32, bf16 = jnp.float32, jnp.bfloat16
    shape = jax.ShapeDtypeStruct
    vmem = pl.BlockSpec(memory_space=pltpu.VMEM)
    dma = pltpu.SemaphoreType.DMA
    messages = 2 * (31 * UNITS + 25)
    gin, gup, gdn, eup, edn = pl.pallas_call(
        functools.partial(kernel, factor),
        out_shape=(
            shape((rows, width), bf16),
            shape((shard, both), f32),
            shape((shard, both), f32),
            shape((shard, 128), f32),
            shape((2, BLOCKS, 128), f32),
        ),
        in_specs=[vmem] * 4,
        out_specs=(vmem,) * 5,
        scratch_shapes=[
            pltpu.VMEM((2, 4 * rows, width), bf16),
            pltpu.VMEM((2, width, 4 * rows), bf16),
            pltpu.VMEM((2 * 32 * UNITS, 16, 128), bf16),
            pltpu.VMEM((2, width, hidden), bf16),
            pltpu.VMEM((4 * rows, max(hidden, width)), f32),
            pltpu.VMEM((4 * rows, hidden), bf16),
            pltpu.VMEM((4 * rows, hidden), bf16),
            pltpu.VMEM((2 * 32 * UNITS, 16, 128), f32),
            pltpu.VMEM((messages, 16, 128), bf16),
            pltpu.VMEM((messages, 16, 128), bf16),
            pltpu.VMEM((2, rows, width), f32),
            pltpu.VMEM((2, 16 + rows // 2, width), bf16),
            pltpu.VMEM((2, 16 + rows // 2, width), bf16),
            pltpu.VMEM((2, 2, UNITS, 16, 128), f32),
            pltpu.VMEM((STEPS + 1, BLOCKS, 128), f32),
            pltpu.VMEM((STEPS + 1, BLOCKS, 128), f32),
            pltpu.VMEM((shard, 128), f32),
            pltpu.VMEM((shard, 128), f32),
            dma((2, 2)),
            dma((2, 2)),
            dma((2, 2)),
            dma((2, 2)),
            dma((2,)),
            dma((2,)),
            dma((2, PARTS, STEPS)),
            dma((2, PARTS, STEPS)),
            dma((2, PARTS, STEPS)),
            dma((2, PARTS, STEPS)),
            dma((2, PARTS)),
            dma((2, PARTS)),
            dma((2,)),
            dma((2,)),
            dma((2,)),
            dma((2,)),
            dma((STEPS + 1,)),
            dma((STEPS + 1,)),
            dma,
            dma,
        ],
        compiler_params=pltpu.CompilerParams(
            collective_id=0, has_side_effects=True, vmem_limit_bytes=60 * 2**20
        ),
        name="step",
    )(inputs, out_cotangent, up_proj, down_proj.T)
    return gin, gup, gdn.T, eup[:, 0], edn.reshape((both,))


def solution(mesh):
    return jax.shard_map(
        body,
        mesh=mesh,
        in_specs=(
            P(("rep", "fs", "tp"), None),
            P("fs", "tp"),
            P("tp", "fs"),
            P(("rep", "fs", "tp"), None),
        ),
        out_specs=(P(("rep", "fs", "tp"), None), P("fs", "tp"), P("tp", "fs"), P("fs"), P("tp")),
        check_vma=False,
    )
```

time: 117 us -> 96.4 us (0.82)
  Pallas kernels: 111 us -> 89.7 us
    pallas_call x1, Pallas kernels: 111 us -> 89.7 us  [body(): pl.pallas_call(functools.partial(kernel, factor), out_shape=(shape((rows,...]
where the time goes in v2:
time: 96.4 us; the launch traced here: 96 us
  Pallas kernels  89.7 us (93%)
  local copies, waits for them, and re-layouts  5.61 us (6%)
    pallas_call x1, Pallas kernels, body(): pl.pallas_call(functools.partial(kernel, factor), out_shape=(shape((rows,...  89.7 us
    unnamed x10, local copies, waits for them, and re-layouts  4.26 us

profile of v2, /device:TPU:0, one launch (start us, length us, event | category | flops | bytes accessed | tf_op | source)
XLA Modules:
  0.0 96.0 jit_solution(15154897961842827405)
XLA Ops:
  0.6 89.7 %step.1 = (bf16[256,1024]{1,0:T(8,128)(2,1)}, f32[32,2048]{1,0:T(8,128)}, f32[32,2048]{1,0:T(8,128)}, f32[32,128]{1,0:T(8,128)}, f32[2,8,128]{2,1,0:T(8,128)}) custom-call(bf16[256,1024]{1,0:T(8,128)(2,1)} %x_ref.1, bf16[256,1024]{1,0:T(8,128)(2,1)} %c_ref.1, bf16[32,2048]{1,0:T(8,128)(2,1)} %u_ref.1, bf16[32,2048]{1,0:T(8,128)(2,1)} %bitcast.4), custom_call_target="tpu_custom_call" | custom-call | tf_op jit(solution)/shard_map/step/pallas_call | solution.py:494
  90.3 1.3 %slice_reduce_fusion = f32[32]{0:T(128)} fusion(f32[32,128]{1,0:T(8,128)} %get-tuple-element.13), kind=kLoop, calls=%fused_computation | loop fusion | bytes 256 | tf_op jit(solution)/shard_map/slice | solution.py:550
  91.7 0.0 copy-start.1
  91.7 1.9 %copy.13 = bf16[256,1024]{1,0:T(8,128)(2,1)} copy(bf16[256,1024]{1,0:T(8,128)(2,1)} %get-tuple-element.20) | data formatting | bytes 1048576
  93.6 0.0 copy-done.1
  93.6 0.0 copy-start
  93.6 0.7 copy.14
  94.3 0.3 copy-done
  94.7 0.0 copy-start.2
  94.7 0.7 copy.15
  95.4 0.0 copy-done.2
  95.4 0.6 copy.16
Async XLA Ops:
  91.7 1.9 %copy-start.1 = (f32[32,2048]{1,0:T(8,128)S(1)}, f32[32,2048]{1,0:T(8,128)}, u32[]{:S(2)}) copy-start(f32[32,2048]{1,0:T(8,128)} %get-tuple-element.21) | copy-start | bytes 786436
  93.6 1.0 %copy-start = (f32[32,2048]{1,0:T(8,128)S(1)}, f32[32,2048]{1,0:T(8,128)}, u32[]{:S(2)}) copy-start(f32[32,2048]{1,0:T(8,128)} %get-tuple-element.12) | copy-start | bytes 786436
  94.7 0.7 copy-start.2

commit v3 on v2

--- a/solution.py
+++ b/solution.py
@@ -71,8 +71,7 @@
     u_ref,
     d_ref,
     gin_ref,
-    gup_ref,
-    gdn_ref,
+    grad_ref,
     eup_ref,
     edn_ref,
     tok,
@@ -89,10 +88,9 @@
     pair_out,
     pair_in,
     outs,
+    gin,
     ebuf,
-    esum,
-    eup_own,
-    eup_in,
+    eup,
     tok_s,
     tok_r,
     fwd_s,
@@ -113,6 +111,7 @@
     e_r,
     eu_s,
     eu_r,
+    out_s,
 ):
     rep, fs, tp = lax.axis_index("rep"), lax.axis_index("fs"), lax.axis_index("tp")
     mine = bits_of(fs)
@@ -120,6 +119,10 @@
     sibling = {"tp": 1 - tp}
     pair = {"rep": 1 - rep, "fs": partners_of(fs)[0]}
     twin = {"rep": 1 - rep}
+    cross = {"rep": 1 - rep, "tp": 1 - tp}
+    z, y, x = fs // 16, (fs // 4) % 4, fs % 4
+    far_x = {"fs": fs + (x + 2) % 4 - x}
+    far_y = {"fs": fs + 4 * ((y + 2) % 4 - y)}
     rows, width = x_ref.shape
     shard = u_ref.shape[0]
     hidden = u_ref.shape[1] // 2
@@ -157,7 +160,7 @@
         return m * UNITS * 32 + STARTS[m][p] * 32
 
     barrier = pltpu.get_barrier_semaphore()
-    for device in near + [sibling, pair, twin]:
+    for device in near + [sibling, pair, twin, cross, far_x, far_y]:
         pl.semaphore_signal(barrier, inc=1, device_id=device, device_id_type=MESH)
 
     for m in range(2):
@@ -169,7 +172,7 @@
                     row * 16 : row * 16 + 16, pl.ds(pl.multiple_of(base + block * 128, 128), 128)
                 ]
 
-    pl.semaphore_wait(barrier, STEPS + 3)
+    pl.semaphore_wait(barrier, STEPS + 6)
 
     pending = []
 
@@ -261,7 +264,7 @@
         )
 
     def chunks(count, size):
-        step = min(count, 4) * size
+        step = min(count, 2) * size
         return count * size // step, step
 
     def highest(m, p, k):
@@ -419,66 +422,111 @@
         start(twin_copy(m, p))
         return value
 
+    def output(i, src, dst):
+        copy = pltpu.make_async_copy(src, dst, out_s.at[i])
+        copy.start()
+        return copy
+
     sums = []
     for p in all_parts:
         value = finish(1, p)
         for i in range(SIZES[1][p]):
             sums.append(jnp.sum(value[i] * value[i], axis=0, keepdims=True))
     for i in range(BLOCKS):
-        ebuf[0, i : i + 1, :] = sums[2 * i] + sums[2 * i + 1]
-
-    def energy_copy(k):
-        device = near[k] if k < STEPS else twin
-        return remote(ebuf.at[k], esum.at[k], e_s.at[k], e_r.at[k], device)
+        ebuf[0, 0, i : i + 1, :] = sums[2 * i] + sums[2 * i + 1]
+
+    rounds = ((near[3], near[4], far_x), (near[1], near[2], far_y), (near[0], twin, pair))
+
+    def energy_copy(k, i):
+        return remote(ebuf.at[k, 0], ebuf.at[k, 1 + i], e_s.at[k, i], e_r.at[k, i], rounds[k][i])
+
+    def energy_begin(k):
+        for i in range(3):
+            start(energy_copy(k, i))
 
     def energy_step(k):
-        energy_copy(k).wait_recv()
-        ebuf[k + 1] = ebuf[k] + esum[k]
-        start(energy_copy(k + 1))
-
-    start(energy_copy(0))
+        for i in range(3):
+            energy_copy(k, i).wait_recv()
+        ebuf[k + 1, 0] = (ebuf[k, 0] + ebuf[k, 1]) + (ebuf[k, 2] + ebuf[k, 3])
+        energy_begin(k + 1)
+
+    energy_begin(0)
     reduce_step(0, 3)
     energy_step(0)
+    squares = [jnp.zeros((16, 128), f32), jnp.zeros((16, 128), f32)]
     for p in all_parts:
-        finish(0, p)
+        value = finish(0, p)
+        for i in range(SIZES[0][p]):
+            row = (STARTS[0][p] + i) % 2
+            squares[row] = squares[row] + value[i] * value[i]
+    for row in range(2):
+        eup[0, row * 16 : row * 16 + 16] = squares[row]
+    row_copies = [
+        start(remote(eup.at[0], eup.at[1 + i], eu_s.at[i], eu_r.at[i], device))
+        for i, device in enumerate((sibling, twin, cross))
+    ]
     energy_step(1)
     for q in range(pieces):
         pair_copy(q).wait_recv()
         s = slice(q * chunk, (q + 1) * chunk)
         scale = pair_in[q, 0:16].astype(f32)[0:1]
-        gin_ref[s] = (pre[s] + decode(pair_in[q, 16 : 16 + chunk], scale)).astype(bf16)
-    energy_step(2)
-
-    def write(m, ref):
-        for p in all_parts:
-            twin_copy(m, p).wait_recv()
+        gin[s] = (pre[s] + decode(pair_in[q, 16 : 16 + chunk], scale)).astype(bf16)
+    outputs = [output(0, gin, gin_ref)]
+    for p in all_parts:
+        twin_copy(1, p).wait_recv()
+    outputs.append(output(1, outs.at[1], grad_ref.at[1]))
+    for i in range(3):
+        energy_copy(2, i).wait_recv()
+    ebuf[3, 0] = (ebuf[2, 0] + ebuf[2, 1]) * (1.0 / width)
+    ebuf[3, 1] = (ebuf[2, 2] + ebuf[2, 3]) * (1.0 / width)
+    outputs.append(output(2, ebuf.at[3, 0], edn_ref.at[rep]))
+    outputs.append(output(3, ebuf.at[3, 1], edn_ref.at[1 - rep]))
+    for p in all_parts:
+        twin_copy(0, p).wait_recv()
+    outputs.append(output(4, outs.at[0], grad_ref.at[0]))
+    for copy in row_copies:
+        copy.wait_recv()
+    outputs.append(output(5, eup, eup_ref))
+    for copy in pending:
+        copy.wait_send()
+    for copy in outputs:
+        copy.wait()
+
+
+def layout(
+    gin_ref, grad_ref, eup_ref, edn_ref, gin_out, gup_out, gdn_out, eup_out, edn_out,
+    gin, grad, eup, edn, both, row, in_s, out_s,
+):
+    pairs = ((gin_ref, gin), (grad_ref.at[1], grad.at[1]), (grad_ref.at[0], grad.at[0]), (eup_ref, eup), (edn_ref, edn))
+    loads = [pltpu.make_async_copy(a, b, in_s.at[i]) for i, (a, b) in enumerate(pairs)]
+    for copy in loads:
+        copy.start()
+    stores = []
+
+    def store(i, src, dst):
+        copy = pltpu.make_async_copy(src, dst, out_s.at[i])
+        copy.start()
+        stores.append(copy)
+
+    half = gup_out.shape[1] // 2
+    loads[3].wait()
+    total = (eup[0] + eup[1]) + (eup[2] + eup[3])
+    row[...] = jnp.sum(total.T, axis=0) * (1.0 / (4 * half))
+    loads[4].wait()
+    store(3, row, eup_out)
+    store(4, edn, edn_out)
+    loads[0].wait()
+    store(0, gin, gin_out)
+    for m, load, out in ((1, 1, gdn_out), (0, 2, gup_out)):
+        loads[load].wait()
         for r in range(2):
             for u in range(UNITS):
-                block, row = divmod(u, 2)
-                left = r * hidden + block * 128
-                ref[row * 16 : row * 16 + 16, left : left + 128] = outs[m, r, u]
-
-    write(1, gdn_ref)
-    energy_step(3)
-    energy_step(4)
-    write(0, gup_ref)
-    for row in range(2):
-        squares = jnp.zeros((16, 128), f32)
-        for r in range(2):
-            for block in range(BLOCKS):
-                value = outs[0, r, 2 * block + row]
-                squares = squares + value * value
-        eup_own[row * 16 : row * 16 + 16, :] = jnp.broadcast_to(
-            jnp.sum(squares, axis=1, keepdims=True), (16, 128)
-        )
-    up_copy = start(remote(eup_own, eup_in, eu_s, eu_r, sibling))
-    energy_copy(STEPS).wait_recv()
-    edn_ref[rep] = ebuf[STEPS] * (1.0 / width)
-    edn_ref[1 - rep] = esum[STEPS] * (1.0 / width)
-    up_copy.wait_recv()
-    eup_ref[...] = (eup_own[...] + eup_in[...]) * (1.0 / (hidden * 4))
-    for copy in pending:
-        copy.wait_send()
+                block, top = divmod(u, 2)
+                left = r * half + block * 128
+                both[m, top * 16 : top * 16 + 16, left : left + 128] = grad[m, r, u]
+        store(load, both.at[m], out)
+    for copy in stores:
+        copy.wait()
 
 
 def body(inputs, up_proj, down_proj, out_cotangent):
@@ -491,17 +539,17 @@
     vmem = pl.BlockSpec(memory_space=pltpu.VMEM)
     dma = pltpu.SemaphoreType.DMA
     messages = 2 * (31 * UNITS + 25)
-    gin, gup, gdn, eup, edn = pl.pallas_call(
+    anywhere = pl.BlockSpec(memory_space=pl.ANY)
+    raw = pl.pallas_call(
         functools.partial(kernel, factor),
         out_shape=(
             shape((rows, width), bf16),
-            shape((shard, both), f32),
-            shape((shard, both), f32),
-            shape((shard, 128), f32),
+            shape((2, 2, UNITS, 16, 128), f32),
+            shape((4, shard, 128), f32),
             shape((2, BLOCKS, 128), f32),
         ),
         in_specs=[vmem] * 4,
-        out_specs=(vmem,) * 5,
+        out_specs=(anywhere,) * 4,
         scratch_shapes=[
             pltpu.VMEM((2, 4 * rows, width), bf16),
             pltpu.VMEM((2, width, 4 * rows), bf16),
@@ -517,10 +565,9 @@
             pltpu.VMEM((2, 16 + rows // 2, width), bf16),
             pltpu.VMEM((2, 16 + rows // 2, width), bf16),
             pltpu.VMEM((2, 2, UNITS, 16, 128), f32),
-            pltpu.VMEM((STEPS + 1, BLOCKS, 128), f32),
-            pltpu.VMEM((STEPS + 1, BLOCKS, 128), f32),
-            pltpu.VMEM((shard, 128), f32),
-            pltpu.VMEM((shard, 128), f32),
+            pltpu.VMEM((rows, width), bf16),
+            pltpu.VMEM((4, 4, BLOCKS, 128), f32),
+            pltpu.VMEM((4, shard, 128), f32),
             dma((2, 2)),
             dma((2, 2)),
             dma((2, 2)),
@@ -537,17 +584,41 @@
             dma((2,)),
             dma((2,)),
             dma((2,)),
-            dma((STEPS + 1,)),
-            dma((STEPS + 1,)),
-            dma,
-            dma,
+            dma((3, 3)),
+            dma((3, 3)),
+            dma((3,)),
+            dma((3,)),
+            dma((6,)),
         ],
         compiler_params=pltpu.CompilerParams(
             collective_id=0, has_side_effects=True, vmem_limit_bytes=60 * 2**20
         ),
         name="step",
     )(inputs, out_cotangent, up_proj, down_proj.T)
-    return gin, gup, gdn.T, eup[:, 0], edn.reshape((both,))
+    gin, gup, gdn, eup, edn = pl.pallas_call(
+        layout,
+        out_shape=(
+            shape((rows, width), bf16),
+            shape((shard, both), f32),
+            shape((shard, both), f32),
+            shape((shard,), f32),
+            shape((2, BLOCKS, 128), f32),
+        ),
+        in_specs=[anywhere] * 4,
+        out_specs=(anywhere,) * 5,
+        scratch_shapes=[
+            pltpu.VMEM((rows, width), bf16),
+            pltpu.VMEM((2, 2, UNITS, 16, 128), f32),
+            pltpu.VMEM((4, shard, 128), f32),
+            pltpu.VMEM((2, BLOCKS, 128), f32),
+            pltpu.VMEM((2, shard, both), f32),
+            pltpu.VMEM((shard,), f32),
+            dma((5,)),
+            dma((5,)),
+        ],
+        name="layout",
+    )(*raw)
+    return gin, gup, gdn.T, eup, edn.reshape((both,))
 
 
 def solution(mesh):

time: 96.4 us -> 86.1 us (0.89)
  local copies, waits for them, and re-layouts: 5.61 us -> 0 us
  Pallas kernels: 89.7 us -> 84.6 us
    pallas_call x1, Pallas kernels: 89.7 us -> 82.3 us  [body(): pl.pallas_call(functools.partial(kernel, factor), out_shape=(shape((rows,...]
    unnamed x10 -> x0, local copies, waits for them, and re-layouts: 4.26 us -> none
    pallas_call x0 -> x1, Pallas kernels: none -> 2.33 us  [body(): pl.pallas_call(layout, out_shape=(shape((rows, width), bf16), shape((shar...]
    slice x1 -> x0, local copies, waits for them, and re-layouts: 1.34 us -> none  [body(): return (gin, gup, gdn.T, eup[:, 0], edn.reshape((both,)))]
where the time goes in v3:
time: 86.1 us; the launch traced here: 85.4 us
  Pallas kernels  84.6 us (98%)
    pallas_call x1, Pallas kernels, body(): pl.pallas_call(functools.partial(kernel, factor), out_shape=(shape((rows,...  82.3 us
    pallas_call x1, Pallas kernels, body(): pl.pallas_call(layout, out_shape=(shape((rows, width), bf16), shape((shar...  2.33 us

profile of v3, /device:TPU:0, one launch (start us, length us, event | category | flops | bytes accessed | tf_op | source)
XLA Modules:
  0.0 85.4 jit_solution(155005994314023462)
XLA Ops:
  0.6 82.3 %step.1 = (bf16[256,1024]{1,0:T(8,128)(2,1)}, f32[2,2,16,16,128]{4,3,2,1,0:T(8,128)}, f32[4,32,128]{2,1,0:T(8,128)}, f32[2,8,128]{2,1,0:T(8,128)}) custom-call(bf16[256,1024]{1,0:T(8,128)(2,1)} %x_ref.1, bf16[256,1024]{1,0:T(8,128)(2,1)} %c_ref.1, bf16[32,2048]{1,0:T(8,128)(2,1)} %u_ref.1, bf16[32,2048]{1,0:T(8,128)(2,1)} %bitcast.3), custom_call_target="tpu_custom_call" | custom-call | tf_op jit(solution)/shard_map/step/pallas_call | solution.py:543
  82.9 2.3 %layout.1 = (bf16[256,1024]{1,0:T(8,128)(2,1)}, f32[32,2048]{1,0:T(8,128)}, f32[32,2048]{1,0:T(8,128)}, f32[32]{0:T(128)}, f32[2,8,128]{2,1,0:T(8,128)}) custom-call(bf16[256,1024]{1,0:T(8,128)(2,1)} %get-tuple-element.14.gin_ref, f32[2,2,16,16,128]{4,3,2,1,0:T(8,128)} %get-tuple-element.15.grad_ref, f32[4,32,128]{2,1,0:T(8,128)} %get-tuple-element.16.eup_ref, ...), custom_call_target="tpu_custom_call" | custom-call | tf_op jit(solution)/shard_map/layout/pallas_call | solution.py:598
